TPU v7x, 32 devices: a whole 2x2x4 slice. The times are simulated.
32 devices in a mesh: grp: 2 (over y), ep: 4 (over z), tp: 4 (over x, core).
Axes of the slice: x: 2, y: 2, z: 4, core: 2. Of those that a mesh axis runs over, the one named last changes fastest.
Arguments:
- mixer_input: bfloat16 [4096, 2048], P(('grp', 'ep', 'tp')), parts along dimension 0, may hold values from -8 to 8
- forget_cumsum: float32 [8, 4096], P('tp', 'grp'), parts along dimension 1, may hold values from -259 to 0, as said below
- mixer_gain: float32 [2048], replicated, may hold values from 0.1 to 1.9
- query_weight: bfloat16 [2048, 1024], P(None, 'tp'), may hold values from -6 to 6
- key_weight: bfloat16 [2048, 1024], P(None, 'tp'), may hold values from -6 to 6
- value_weight: bfloat16 [2048, 1024], P(None, 'tp'), may hold values from -0.125 to 0.125
- out_weight: bfloat16 [1024, 2048], P('tp'), may hold values from -0.1875 to 0.1875
- post_gain: float32 [2048], replicated, may hold values from 0.1 to 1.9
- expert_input: bfloat16 [4096, 2048], P(('grp', 'ep', 'tp')), parts along dimension 0, may hold values from -6 to 6
- expert_gain: float32 [2048], replicated, may hold values from 0.1 to 1.9
- routes: int32 [4096, 2], P(('grp', 'ep', 'tp')), parts along dimension 0, may hold values from 0 to 3, all different within a row; in each aligned block of 128 rows (0 to 127, 128 to 255, ...) at most 72 rows name the same one
- route_weight: float32 [4096, 2], P(('grp', 'ep', 'tp')), parts along dimension 0, may hold values from 0.2 to 1
- expert_gate: bfloat16 [4, 2048, 2048], P('ep', None, 'tp'), may hold values from -0.125 to 0.125
- expert_upward: bfloat16 [4, 2048, 2048], P('ep', None, 'tp'), may hold values from -0.125 to 0.125
- expert_down: bfloat16 [4, 2048, 2048], P('ep', 'tp'), may hold values from -0.125 to 0.125
Outputs:
- mixer_output: bfloat16 [4096, 2048], P(('grp', 'ep', 'tp')), parts along dimension 0
- expert_output: bfloat16 [4096, 2048], P(('grp', 'ep', 'tp')), parts along dimension 0
There are 2 independent parts, one for each index of `grp`. A program takes and returns all parts, laid end to end along the dimension named above; an argument that names none is the same for every part. Nothing has to cross between parts.
Inputs may be any that keep to these rules, and one draw needn't show every extreme that they name: `forget_cumsum`: each head's row never rises along positions. `routes`: A row names 2 different experts. Within the rows of one device (aligned blocks of 128 rows) no expert is named by more than 72 rows, and in every draw some expert is named by exactly 72 rows of some block.
All inputs are finite; a program needn't handle non-finite values.
Results may differ from a plain program's by a relative error of at most 0.012.
Values may be sent and summed in bfloat16 or wider, within the bound.
A program may use at most 128 MiB of HBM per device.

v0:
```python
import jax
import jax.numpy as jnp
from jax import lax
from jax.sharding import PartitionSpec as P

EPS = 1e-06
MASKED = -1e30


def normalize(row_block, gain):
    values = row_block.astype(jnp.float32)
    inverse = lax.rsqrt(jnp.mean(values * values, axis=-1, keepdims=True) + EPS)
    return values * inverse * gain


def on_device(
    mixer_input,
    forget_cumsum,
    mixer_gain,
    query_weight,
    key_weight,
    value_weight,
    out_weight,
    post_gain,
    expert_input,
    expert_gain,
    routes,
    route_weight,
    expert_gate,
    expert_upward,
    expert_down,
):
    ep_count = lax.axis_size("ep")
    tp_count = lax.axis_size("tp")
    mix_rows = mixer_input.shape[0]
    feature_width = mixer_input.shape[1]
    heads_local = forget_cumsum.shape[0]
    head_width = query_weight.shape[1]
    head_dim = head_width // heads_local
    group_span = mix_rows * tp_count
    first_pos = lax.axis_index("ep") * group_span
    last_pos = first_pos + group_span - 1
    score_scale = head_dim ** (-0.5)
    normed = normalize(mixer_input, mixer_gain).astype(jnp.bfloat16)
    segment = lax.all_gather(normed, "tp", axis=0, tiled=True)
    products = [
        jnp.dot(segment, weight, preferred_element_type=jnp.float32)
        for weight in (query_weight, key_weight, value_weight)
    ]
    joined = jnp.concatenate(products, axis=1).astype(jnp.bfloat16)
    queries = joined[:, :head_width].reshape(group_span, heads_local, head_dim)
    key_rows = joined[:, head_width : 2 * head_width]
    value_rows = joined[:, 2 * head_width :]
    query_pos = first_pos + jnp.arange(group_span, dtype=jnp.int32)
    query_gate = lax.dynamic_slice_in_dim(forget_cumsum, first_pos, group_span, 1)

    def key_block(state, key_part, value_part, key_first):
        key_count = key_part.shape[0]

        def compute(current):
            running_max, running_sum, running_acc = current
            key_heads = key_part.reshape(key_count, heads_local, head_dim)
            value_heads = value_part.reshape(key_count, heads_local, head_dim)
            key_gate = lax.dynamic_slice_in_dim(forget_cumsum, key_first, key_count, 1)
            scores = (
                jnp.einsum("qhd,khd->hqk", queries, key_heads, preferred_element_type=jnp.float32)
                * score_scale
            )
            scores = scores + query_gate[:, :, None] - key_gate[:, None, :]
            key_pos = key_first + jnp.arange(key_count, dtype=jnp.int32)
            visible = (key_pos[None, :] <= query_pos[:, None])[None]
            scores = jnp.where(visible, scores, MASKED)
            new_max = jnp.maximum(running_max, jnp.max(scores, axis=-1))
            weights = jnp.where(visible, jnp.exp(scores - new_max[..., None]), 0.0)
            rescale = jnp.exp(running_max - new_max)
            running_sum = running_sum * rescale + jnp.sum(weights, axis=-1)
            running_acc = running_acc * rescale[..., None] + jnp.einsum(
                "hqk,khd->hqd",
                weights.astype(jnp.bfloat16),
                value_heads,
                preferred_element_type=jnp.float32,
            )
            return (new_max, running_sum, running_acc)

        def keep_state(current):
            return current

        return lax.cond(key_first > last_pos, keep_state, compute, state)

    initial = (
        jnp.full((heads_local, group_span), MASKED, jnp.float32),
        jnp.zeros((heads_local, group_span), jnp.float32),
        jnp.zeros((heads_local, group_span, head_dim), jnp.float32),
    )
    key_part = lax.all_gather(key_rows, "ep", axis=0, tiled=True)
    value_part = lax.all_gather(value_rows, "ep", axis=0, tiled=True)
    row_count = key_part.shape[0]
    block_size = 512
    block_count = row_count // block_size

    def advance_increment(block_index, current):
        offset = block_index * block_size
        return key_block(
            current,
            lax.dynamic_slice_in_dim(key_part, offset, block_size, 0),
            lax.dynamic_slice_in_dim(value_part, offset, block_size, 0),
            offset,
        )

    running_max, running_sum, running_acc = lax.fori_loop(
        0, block_count, advance_increment, initial
    )
    attended = (running_acc / running_sum[..., None]).astype(jnp.bfloat16)
    attended = attended.transpose(1, 0, 2).reshape(group_span, head_width)
    moe_rows, top_count = routes.shape
    experts_local = expert_gate.shape[0]
    experts_all = ep_count * experts_local
    capacity = (moe_rows * top_count * 9 + 8 * experts_all - 1) // (8 * experts_all)
    slots_all = experts_all * capacity
    normed_moe = normalize(expert_input, expert_gain).astype(jnp.bfloat16)
    flat_routes = routes.reshape(-1)
    member = (flat_routes[:, None] == jnp.arange(experts_all, dtype=jnp.int32)[None, :]).astype(
        jnp.int32
    )
    before = jnp.cumsum(member, axis=0) - member
    slot_rank = jnp.sum(before * member, axis=1)
    slot_index = (flat_routes * capacity + slot_rank).reshape(moe_rows, top_count)
    slot_ids = jnp.arange(slots_all, dtype=jnp.int32)
    choosers = [
        (slot_index[:, which][:, None] == slot_ids[None, :]).astype(jnp.bfloat16)
        for which in range(top_count)
    ]
    dispatch = choosers[0]
    which = 1
    dispatch = dispatch + choosers[which]
    outgoing = lax.dot_general(
        dispatch, normed_moe, (((0,), (0,)), ((), ())), preferred_element_type=jnp.float32
    ).astype(jnp.bfloat16)
    outgoing = outgoing.reshape(ep_count, experts_local, capacity, feature_width)
    copies = jnp.broadcast_to(
        outgoing[:, None], (ep_count, tp_count, experts_local, capacity, feature_width)
    )
    copies = copies.reshape(ep_count * tp_count, experts_local, capacity, feature_width)
    stacked = lax.all_to_all(copies, ("ep", "tp"), split_axis=0, concat_axis=0, tiled=True).reshape(
        ep_count, tp_count, experts_local, capacity, feature_width
    )
    shard_axis = 1
    expert_rows_count = ep_count * experts_local * capacity

    def expert_term(block_index):
        selected = lax.dynamic_index_in_dim(stacked, block_index, shard_axis, keepdims=False)
        gate_proj = jnp.einsum(
            "secd,edf->secf", selected, expert_gate, preferred_element_type=jnp.float32
        )
        upward = jnp.einsum(
            "secd,edf->secf", selected, expert_upward, preferred_element_type=jnp.float32
        )
        hidden = (jax.nn.silu(gate_proj) * upward).astype(jnp.bfloat16)
        result = jnp.einsum(
            "secf,efd->secd", hidden, expert_down, preferred_element_type=jnp.float32
        )
        return result.reshape(expert_rows_count, feature_width)

    selected = attended
    mixer_sum = lax.psum_scatter(
        jnp.dot(selected, out_weight, preferred_element_type=jnp.float32).astype(jnp.bfloat16),
        "tp",
        scatter_dimension=0,
        tiled=True,
    ).astype(jnp.float32)
    first_block = jnp.int32(0) // expert_rows_count
    pieces = [
        expert_term(first_block + offset)
        for offset in range(expert_rows_count * lax.axis_size("tp") // expert_rows_count)
    ]
    expert_sum = lax.psum_scatter(
        jnp.concatenate(pieces, axis=0).astype(jnp.bfloat16), "tp", scatter_dimension=0, tiled=True
    )
    mixer_output = normalize(mixer_sum, post_gain).astype(jnp.bfloat16)
    results = expert_sum.reshape(ep_count, experts_local, capacity, feature_width)
    returned = lax.all_to_all(results, "ep", split_axis=0, concat_axis=0, tiled=True).reshape(
        slots_all, feature_width
    )
    combined = jnp.zeros((moe_rows, feature_width), jnp.float32)
    for which in range(top_count):
        picked = jnp.dot(choosers[which], returned, preferred_element_type=jnp.float32)
        combined = combined + route_weight[:, which : which + 1] * picked
    expert_output = combined.astype(jnp.bfloat16)
    return (mixer_output, expert_output)


def solution(mesh):
    in_specs = (
        P(("grp", "ep", "tp"), None),
        P("tp", "grp"),
        P(),
        P(None, "tp"),
        P(None, "tp"),
        P(None, "tp"),
        P("tp", None),
        P(),
        P(("grp", "ep", "tp"), None),
        P(),
        P(("grp", "ep", "tp"), None),
        P(("grp", "ep", "tp"), None),
        P("ep", None, "tp"),
        P("ep", None, "tp"),
        P("ep", "tp", None),
    )
    out_specs = (P(("grp", "ep", "tp"), None), P(("grp", "ep", "tp"), None))
    return jax.shard_map(
        on_device, mesh=mesh, in_specs=in_specs, out_specs=out_specs, check_vma=False
    )
```

profile of v0, /device:TPU:26, one launch (start us, length us, event | category | flops | bytes accessed | tf_op | source)
XLA Modules:
  0.0 282.3 jit_solution(11052232415735645723)
XLA Ops:
  7.2 0.9 copy.79
  8.3 0.1 eq.55
  8.4 1.2 reduce-window.6
  10.1 0.1 reduce_sum.53
  10.3 0.7 multiply_add_fusion.1
  11.0 1.2 fusion.97
  12.2 1.6 convolution_convert_fusion.1
  13.8 2.8 broadcast_in_dim.67
  16.6 6.1 %all-to-all-start = ((bf16[16,1,72,2048]{3,2,1,0:T(8,128)(2,1)}), bf16[16,1,72,2048]{3,2,1,0:T(8,128)(2,1)}, u32[]{:S(2)}, u32[]{:S(2)}) async-start(bf16[16,1,72,2048]{3,2,1,0:T(8,128)(2,1)} %bitcast.288), calls=%async_computation.1 | async-start | bytes 9437184 | tf_op jit(solution)/shard_map/all_to_all | solution.py:144
  22.8 0.2 fusion.91
  23.0 1.0 fusion.93
  24.1 44.8 %all-gather.4.cloned.1.call-done = bf16[512,2048]{1,0:T(8,128)(2,1)} async-done(((bf16[128,2048]{1,0:T(8,128)(2,1)}), bf16[512,2048]{1,0:T(8,128)(2,1)}) %all-gather.4.cloned.1.call-update) | async-done | bytes 2097168 | tf_op jit(solution)/shard_map/all_gather | solution.py:45
  68.8 3.3 %convolution_convert_fusion.8 = bf16[512,256]{1,0:T(8,128)(2,1)} fusion(bf16[512,2048]{1,0:T(8,128)(2,1)} %all-gather.4.cloned.1.call-done, bf16[2048,256]{1,0:T(8,128)(2,1)} %param.23), kind=kOutput, calls=%fused_computation.73 | convolution fusion | flops 537001984 | bytes 3407872 | tf_op jit(solution)/shard_map/dot_general | solution.py:47
  72.2 3.0 %convolution_convert_fusion.6 = bf16[512,256]{1,0:T(8,128)(2,1)} fusion(bf16[512,2048]{1,0:T(8,128)(2,1)} %all-gather.4.cloned.1.call-done, bf16[2048,256]{1,0:T(8,128)(2,1)S(1)} %copy-done.7), kind=kOutput, calls=%fused_computation.71 | convolution fusion | flops 537001984 | bytes 3407872 | tf_op jit(solution)/shard_map/dot_general | solution.py:47
  75.3 77.5 %all-to-all-done = bf16[16,1,72,2048]{3,2,1,0:T(8,128)(2,1)} async-done(((bf16[16,1,72,2048]{3,2,1,0:T(8,128)(2,1)}), bf16[16,1,72,2048]{3,2,1,0:T(8,128)(2,1)}, u32[]{:S(2)}, u32[]{:S(2)}) %all-to-all-start) | async-done | bytes 4718624 | tf_op jit(solution)/shard_map/all_to_all | solution.py:144
  152.8 3.7 %fusion.31 = f32[4,1,72,512]{3,2,0,1:T(8,128)} fusion(bf16[1,2048,512]{2,1,0:T(8,128)(2,1)} %param.31, bf16[4,4,1,72,2048]{4,3,1,0,2:T(8,128)(2,1)} %bitcast.13), kind=kOutput, calls=%fused_computation.55 | convolution fusion | flops 603979776 | bytes 3866624 | tf_op jit(solution)/shard_map/secd,edf->secf/dot_general | solution.py:152
  156.5 2.9 %fusion.34 = f32[4,1,72,512]{3,2,0,1:T(8,128)} fusion(bf16[1,2048,512]{2,1,0:T(8,128)(2,1)S(1)} %copy-done.6, bf16[4,4,1,72,2048]{4,3,1,0,2:T(8,128)(2,1)} %bitcast.13), kind=kOutput, calls=%fused_computation.56 | convolution fusion | flops 603979776 | bytes 3866624 | tf_op jit(solution)/shard_map/secd,edf->secf/dot_general | solution.py:152
  159.3 2.9 %fusion.37 = f32[4,1,72,512]{3,2,0,1:T(8,128)} fusion(bf16[1,2048,512]{2,1,0:T(8,128)(2,1)S(1)} %copy-done.6, bf16[4,4,1,72,2048]{4,3,1,0,2:T(8,128)(2,1)} %bitcast.13), kind=kOutput, calls=%fused_computation.57 | convolution fusion | flops 603979776 | bytes 3866624 | tf_op jit(solution)/shard_map/secd,edf->secf/dot_general | solution.py:152
  162.2 3.5 %convolution_convert_fusion.5 = bf16[4,72,2048]{2,1,0:T(8,128)(2,1)S(1)} fusion(bf16[1,512,2048]{2,1,0:T(8,128)(2,1)S(1)} %copy-done, bf16[1,2048,512]{2,1,0:T(8,128)(2,1)} %param.32, bf16[4,4,1,72,2048]{4,3,1,0,2:T(8,128)(2,1)} %bitcast.13, f32[4,1,72,512]{3,2,0,1:T(8,128)} %fusion.31), kind=kOutput, calls=%fused_computation.24 | convolution fusion | flops 1209434112 | bytes 7143424 | tf_op jit(solution)/shard_map/secf,efd->secd/dot_general | solution.py:159
  165.8 4.6 %convolution_convert_fusion.4 = bf16[4,72,2048]{2,1,0:T(8,128)(2,1)} fusion(bf16[1,512,2048]{2,1,0:T(8,128)(2,1)S(1)} %copy-done, bf16[1,2048,512]{2,1,0:T(8,128)(2,1)} %param.32, bf16[4,4,1,72,2048]{4,3,1,0,2:T(8,128)(2,1)} %bitcast.13, f32[4,1,72,512]{3,2,0,1:T(8,128)} %fusion.34), kind=kOutput, calls=%fused_computation.23 | convolution fusion | flops 1209434112 | bytes 7143424 | tf_op jit(solution)/shard_map/secf,efd->secd/dot_general | solution.py:159
  170.4 4.6 %convolution_convert_fusion.3 = bf16[4,72,2048]{2,1,0:T(8,128)(2,1)} fusion(bf16[1,512,2048]{2,1,0:T(8,128)(2,1)S(1)} %copy-done, bf16[1,2048,512]{2,1,0:T(8,128)(2,1)} %param.32, bf16[4,4,1,72,2048]{4,3,1,0,2:T(8,128)(2,1)} %bitcast.13, f32[4,1,72,512]{3,2,0,1:T(8,128)} %fusion.37), kind=kOutput, calls=%fused_computation.22 | convolution fusion | flops 1209434112 | bytes 7143424 | tf_op jit(solution)/shard_map/secf,efd->secd/dot_general | solution.py:159
  175.0 3.6 %fusion.40 = f32[4,1,72,512]{3,2,0,1:T(8,128)} fusion(bf16[1,2048,512]{2,1,0:T(8,128)(2,1)} %param.31, bf16[4,4,1,72,2048]{4,3,1,0,2:T(8,128)(2,1)} %bitcast.13), kind=kOutput, calls=%fused_computation.58 | convolution fusion | flops 603979776 | bytes 3866624 | tf_op jit(solution)/shard_map/secd,edf->secf/dot_general | solution.py:152
  178.6 4.6 %convolution_convert_fusion.2 = bf16[4,72,2048]{2,1,0:T(8,128)(2,1)} fusion(bf16[1,512,2048]{2,1,0:T(8,128)(2,1)S(1)} %copy-done, bf16[1,2048,512]{2,1,0:T(8,128)(2,1)} %param.32, bf16[4,4,1,72,2048]{4,3,1,0,2:T(8,128)(2,1)} %bitcast.13, f32[4,1,72,512]{3,2,0,1:T(8,128)} %fusion.40), kind=kOutput, calls=%fused_computation.21 | convolution fusion | flops 1209434112 | bytes 7143424 | tf_op jit(solution)/shard_map/secf,efd->secd/dot_general | solution.py:159
  183.1 3.8 %pad_maximum_fusion = bf16[1152,2048]{1,0:T(8,128)(2,1)} fusion(bf16[288,2048]{1,0:T(8,128)(2,1)} %bitcast.297, bf16[288,2048]{1,0:T(8,128)(2,1)} %bitcast.296, bf16[288,2048]{1,0:T(8,128)(2,1)} %bitcast.295, bf16[288,2048]{1,0:T(8,128)(2,1)S(1)} %bitcast.294), kind=kLoop, calls=%fused_computation.18 | loop fusion | flops 18874368 | bytes 9437184 | tf_op jit(solution)/shard_map/concatenate | solution.py:177
  187.0 0.2 reduce-scatter.3.cloned.1.call-start
  187.2 0.5 copy-done.2
  187.7 2.6 convolution_convert_fusion.7
  190.3 0.2 copy.76
  190.5 2.3 copy.75
  192.8 2.3 copy.77
  195.1 14.6 %while.18 = (s32[]{:T(128)}, f32[2,512]{1,0:T(2,128)S(1)}, f32[2,512]{1,0:T(2,128)S(1)}, f32[2,512,128]{2,1,0:T(8,128)S(1)}, s32[]{:T(128)}, /*index=5*/bf16[204...) while((s32[]{:T(128)}, f32[2,512]{1,0:T(2,128)S(1)}, ...), condition=%wide.region_6.7_spmd.clone, body=%wide.region_1.6_spmd.clone.sunk | while | flops 274729984 | bytes 10318161 | solution.py:110
  195.2 3.7 %conditional.3 = (f32[2,512]{1,0:T(2,128)S(1)}, f32[2,512]{1,0:T(2,128)S(1)}, f32[2,512,128]{2,1,0:T(8,128)S(1)}) conditional(s32[]{:T(128)} %convert_element_type.155, (s32[]{:T(128)}, s32[]{:T(128)}, bf16[2048,256]{0,1:T(8,128)(2,1)}, bf16[512,2,128]{2,0,1:T(8,128)(2,1)S(1)}, f32[2,512]{1,0:T(2,128)S(1)}, /*index=5*/f32[2,2048]{1,0:T(2,128)S(1)}, ...), branch_computations={%region_2.4_spmd, %region_5.5_spmd} | conditional | flops 274729984 | bytes 10307658 | solution.py:88
  195.2 1.2 constant_dynamic-slice_fusion.1
  196.4 0.2 broadcast_compare_fusion
  196.7 0.8 fusion.151
  197.5 0.4 fusion.3
  197.9 0.9 convolution_add_fusion
  198.9 3.7 %conditional.3 = (f32[2,512]{1,0:T(2,128)S(1)}, f32[2,512]{1,0:T(2,128)S(1)}, f32[2,512,128]{2,1,0:T(8,128)S(1)}) conditional(s32[]{:T(128)} %convert_element_type.155, (s32[]{:T(128)}, s32[]{:T(128)}, bf16[2048,256]{0,1:T(8,128)(2,1)}, bf16[512,2,128]{2,0,1:T(8,128)(2,1)S(1)}, f32[2,512]{1,0:T(2,128)S(1)}, /*index=5*/f32[2,2048]{1,0:T(2,128)S(1)}, ...), branch_computations={%region_2.4_spmd, %region_5.5_spmd} | conditional | flops 274729984 | bytes 10307658 | solution.py:88
  198.9 1.2 constant_dynamic-slice_fusion.1
  200.2 0.2 broadcast_compare_fusion
  200.4 0.8 fusion.151
  201.2 0.4 fusion.3
  201.7 0.9 convolution_add_fusion
  202.7 3.5 %conditional.3 = (f32[2,512]{1,0:T(2,128)S(1)}, f32[2,512]{1,0:T(2,128)S(1)}, f32[2,512,128]{2,1,0:T(8,128)S(1)}) conditional(s32[]{:T(128)} %convert_element_type.155, (s32[]{:T(128)}, s32[]{:T(128)}, bf16[2048,256]{0,1:T(8,128)(2,1)}, bf16[512,2,128]{2,0,1:T(8,128)(2,1)S(1)}, f32[2,512]{1,0:T(2,128)S(1)}, /*index=5*/f32[2,2048]{1,0:T(2,128)S(1)}, ...), branch_computations={%region_2.4_spmd, %region_5.5_spmd} | conditional | flops 274729984 | bytes 10307658 | solution.py:88
  202.7 1.1 constant_dynamic-slice_fusion.1
  203.8 0.2 broadcast_compare_fusion
  204.0 0.8 fusion.151
  204.8 0.4 fusion.3
  205.3 0.9 convolution_add_fusion
  206.2 3.5 %conditional.3 = (f32[2,512]{1,0:T(2,128)S(1)}, f32[2,512]{1,0:T(2,128)S(1)}, f32[2,512,128]{2,1,0:T(8,128)S(1)}) conditional(s32[]{:T(128)} %convert_element_type.155, (s32[]{:T(128)}, s32[]{:T(128)}, bf16[2048,256]{0,1:T(8,128)(2,1)}, bf16[512,2,128]{2,0,1:T(8,128)(2,1)S(1)}, f32[2,512]{1,0:T(2,128)S(1)}, /*index=5*/f32[2,2048]{1,0:T(2,128)S(1)}, ...), branch_computations={%region_2.4_spmd, %region_5.5_spmd} | conditional | flops 274729984 | bytes 10307658 | solution.py:88
  206.2 1.1 constant_dynamic-slice_fusion.1
  207.3 0.2 broadcast_compare_fusion
  207.6 0.8 fusion.151
  208.4 0.4 fusion.3
  208.8 0.9 convolution_add_fusion
  209.8 0.2 copy.78
  210.0 3.5 %convolution_convert_fusion = bf16[512,2048]{1,0:T(8,128)(2,1)} fusion(bf16[512,256]{0,1:T(8,128)(2,1)S(1)} %bitcast.293, bf16[256,2048]{1,0:T(8,128)(2,1)} %param.25), kind=kOutput, calls=%fused_computation.19 | convolution fusion | flops 537919488 | bytes 3407872 | tf_op jit(solution)/shard_map/dot_general | solution.py:166
  213.5 23.6 %reduce-scatter.5.cloned.1.call-done = bf16[288,2048]{1,0:T(8,128)(2,1)} async-done(((bf16[1152,2048]{1,0:T(8,128)(2,1)}), bf16[288,2048]{1,0:T(8,128)(2,1)}) %reduce-scatter.5.cloned.1.call-update) | async-done | bytes 1179664 | tf_op jit(solution)/shard_map/reduce_scatter | solution.py:176
  237.1 5.1 %all-to-all-start.1 = ((bf16[4,1,72,2048]{3,2,1,0:T(8,128)(2,1)}), bf16[4,1,72,2048]{3,2,1,0:T(8,128)(2,1)S(1)}, u32[]{:S(2)}, u32[]{:S(2)}) async-start(bf16[4,1,72,2048]{3,2,1,0:T(8,128)(2,1)} %bitcast.298), calls=%async_computation.3 | async-start | bytes 2359296 | tf_op jit(solution)/shard_map/all_to_all | solution.py:181
  242.2 28.5 %reduce-scatter.3.cloned.1.call-done = bf16[128,2048]{1,0:T(8,128)(2,1)} async-done(((bf16[512,2048]{1,0:T(8,128)(2,1)}), bf16[128,2048]{1,0:T(8,128)(2,1)}) %reduce-scatter.3.cloned.1.call-update) | async-done | bytes 524304 | tf_op jit(solution)/shard_map/reduce_scatter | solution.py:165
  270.7 1.2 fusion.94
  271.9 2.0 fusion.96
  274.0 0.5 convolution_multiply_fusion.1
  274.5 1.3 fusion.10
  (71 shorter events, 1.2 us)
Async XLA Ops:
  7.2 155.0 %copy-start = (bf16[1,512,2048]{2,1,0:T(8,128)(2,1)S(1)}, bf16[1,512,2048]{2,1,0:T(8,128)(2,1)}, u32[]{:S(2)}) copy-start(bf16[1,512,2048]{2,1,0:T(8,128)(2,1)} %param.33) | copy-start | bytes 6291460
  16.6 6.2 %copy-start.1 = (bf16[128,2048]{1,0:T(8,128)(2,1)S(1)}, bf16[128,2048]{1,0:T(8,128)(2,1)}, u32[]{:S(2)}) copy-start(bf16[128,2048]{1,0:T(8,128)(2,1)} %param.19) | copy-start | bytes 1572868
  16.6 6.4 %copy-start.3 = (f32[2048]{0:T(1024)S(1)}, f32[2048]{0:T(1024)}, u32[]{:S(2)}) copy-start(f32[2048]{0:T(1024)} %param.21) | copy-start | bytes 24580
  16.6 136.2 %all-to-all-start = ((bf16[16,1,72,2048]{3,2,1,0:T(8,128)(2,1)}), bf16[16,1,72,2048]{3,2,1,0:T(8,128)(2,1)}, u32[]{:S(2)}, u32[]{:S(2)}) async-start(bf16[16,1,72,2048]{3,2,1,0:T(8,128)(2,1)} %bitcast.288), calls=%async_computation.1 | async-start | bytes 9437184 | tf_op jit(solution)/shard_map/all_to_all | solution.py:144
  22.8 46.1 %all-gather.4.cloned.1.call-start = ((), (), s32[]{:S(2)}) async-start(), calls=%async_computation.4 | async-start | bytes 2621440 | tf_op jit(solution)/shard_map/all_gather | solution.py:45
  24.0 48.2 %copy-start.7 = (bf16[2048,256]{1,0:T(8,128)(2,1)S(1)}, bf16[2048,256]{1,0:T(8,128)(2,1)}, u32[]{:S(2)}) copy-start(bf16[2048,256]{1,0:T(8,128)(2,1)} %param.24) | copy-start | bytes 3145732
  24.0 166.5 %all-gather.6.cloned.1.call-start = ((), (), s32[]{:S(2)}) async-start(), calls=%async_computation.5 | async-start | bytes 1310720 | tf_op jit(solution)/shard_map/all_gather | solution.py:95
  72.1 120.7 %all-gather.8.cloned.1.call-start = ((), (), s32[]{:S(2)}) async-start(), calls=%async_computation.6 | async-start | bytes 1310720 | tf_op jit(solution)/shard_map/all_gather | solution.py:96
  75.2 161.9 %reduce-scatter.5.cloned.1.call-start = ((), (), s32[]{:S(2)}) async-start(), calls=%async_computation.8 | async-start | bytes 5898240 | tf_op jit(solution)/shard_map/reduce_scatter | solution.py:176
  152.8 3.7 %copy-start.6 = (bf16[1,2048,512]{2,1,0:T(8,128)(2,1)S(1)}, bf16[1,2048,512]{2,1,0:T(8,128)(2,1)}, u32[]{:S(2)}) copy-start(bf16[1,2048,512]{2,1,0:T(8,128)(2,1)} %param.31) | copy-start | bytes 6291460
  187.0 0.7 copy-start.2
  187.0 83.7 %reduce-scatter.3.cloned.1.call-start = ((), (), s32[]{:S(2)}) async-start(), calls=%async_computation.7 | async-start | bytes 2621440 | tf_op jit(solution)/shard_map/reduce_scatter | solution.py:165
  213.5 28.7 %copy-start.5 = (f32[128,2]{0,1:T(2,128)S(1)}, f32[128,2]{0,1:T(2,128)}, u32[]{:S(2)}) copy-start(f32[128,2]{0,1:T(2,128)} %param.30) | copy-start | bytes 3076
  213.5 58.4 %copy-start.4 = (f32[2048]{0:T(1024)S(1)}, f32[2048]{0:T(1024)}, u32[]{:S(2)}) copy-start(f32[2048]{0:T(1024)} %param.26) | copy-start | bytes 24580
  237.1 36.8 %all-to-all-start.1 = ((bf16[4,1,72,2048]{3,2,1,0:T(8,128)(2,1)}), bf16[4,1,72,2048]{3,2,1,0:T(8,128)(2,1)S(1)}, u32[]{:S(2)}, u32[]{:S(2)}) async-start(bf16[4,1,72,2048]{3,2,1,0:T(8,128)(2,1)} %bitcast.298), calls=%async_computation.3 | async-start | bytes 2359296 | tf_op jit(solution)/shard_map/all_to_all | solution.py:181
Sparse Core Ops, SparseCore 0:
  25.7 43.1 all-gather.3
  72.3 48.4 all-gather.5
  122.9 36.7 all-gather.7
  187.1 49.9 reduce-scatter.4
  239.5 31.1 reduce-scatter.2
where the time goes:
time: 286 us; the launch traced here: 282 us
  waiting for transfers between devices  174 us (61%)
  matrix products  52.8 us (18%)
  local copies, waits for them, and re-layouts  14.6 us (5%)
  other arithmetic  14.3 us (5%)
  between operations  14 us (5%)
  starting transfers between devices  11.6 us (4%)
    all_to_all x1, waiting for transfers between devices, on_device(): lax.all_to_all(copies, ('ep', 'tp'), split_axis=0, concat_axis=0, tiled=T...  77.5 us
    all_gather x1, waiting for transfers between devices, on_device(): segment = lax.all_gather(normed, 'tp', axis=0, tiled=True)  44.8 us
    reduce_scatter x1, waiting for transfers between devices, on_device(): lax.psum_scatter(jnp.dot(selected, out_weight, preferred_element_type=jnp...  28.5 us
    reduce_scatter x1, waiting for transfers between devices, on_device(): lax.psum_scatter(jnp.concatenate(pieces, axis=0).astype(jnp.bfloat16), 't...  23.6 us
    dot_general x4, matrix products, expert_term(): jnp.einsum('secf,efd->secd', hidden, expert_down, preferred_element_type=...  17.3 us
    dot_general x4, matrix products, expert_term(): jnp.einsum('secd,edf->secf', selected, expert_gate, preferred_element_typ...  13 us
    dot_general x3, matrix products, on_device(): jnp.dot(segment, weight, preferred_element_type=jnp.float32)  8.88 us
    unnamed x20, local copies, waits for them, and re-layouts  6.17 us
  transfers between devices with their start and end apart: 7, of which 4 were waited for; matrix products, arithmetic and copies ran while one was open for 25% of the time, Pallas kernels for 0%

commit v1 on v0

v1 whole, which is shorter than its diff:
```python
import functools

import jax
import jax.numpy as jnp
from jax import lax
from jax.experimental import pallas as pl
from jax.experimental.pallas import tpu as pltpu
from jax.sharding import PartitionSpec as P

EPS = 1e-06
MASKED = -1e30
MESH = pl.DeviceIdType.MESH
F32 = jnp.float32
BF16 = jnp.bfloat16


def normalize(row_block, gain):
    values = row_block.astype(F32)
    inverse = lax.rsqrt(jnp.mean(values * values, axis=-1, keepdims=True) + EPS)
    return values * inverse * gain


def tile_of(width, largest):
    return largest if width % largest == 0 else width


def kernel(
    n_ep,
    head_dim,
    normed_ref,
    outgoing_ref,
    query_gate_ref,
    gate_ref,
    post_gain_ref,
    wq_hbm,
    wk_hbm,
    wv_hbm,
    wo_hbm,
    eg_hbm,
    eu_hbm,
    ed_hbm,
    mixer_ref,
    returned_ref,
    wq,
    wk,
    wv,
    wo,
    eg,
    eu,
    ed,
    seg,
    queries,
    kv,
    rows,
    hid,
    res,
    drec,
    erec,
    fin,
    run_max,
    run_sum,
    run_acc,
    attended,
    mdrec,
    merec,
    w_sem,
    ns,
    nr,
    as_,
    ar,
    bs,
    br,
    cs,
    cr,
    ds,
    dr,
    es,
    er,
    fs,
    fr,
    ks,
    kr,
    ms,
    mr,
):
    me = lax.axis_index("ep")
    t = lax.axis_index("tp")
    hi = t // 2
    lo = t % 2
    lo_peer = 2 * hi + (1 - lo)
    hi_peer = 2 * (1 - hi) + lo
    other_hi = 1 - hi
    mix_rows, width = normed_ref.shape
    head_width = wq.shape[1]
    heads = head_width // head_dim
    span = 4 * mix_rows
    cap = outgoing_ref.shape[1]

    def remote(src, dst, send_sem, recv_sem, where):
        return pltpu.make_async_remote_copy(
            src_ref=src,
            dst_ref=dst,
            send_sem=send_sem,
            recv_sem=recv_sem,
            device_id=where,
            device_id_type=MESH,
        )

    loads = [
        pltpu.make_async_copy(src, dst, w_sem.at[i])
        for i, (src, dst) in enumerate(
            ((wq_hbm, wq), (wk_hbm, wk), (wv_hbm, wv), (wo_hbm, wo), (eg_hbm, eg), (eu_hbm, eu), (ed_hbm, ed))
        )
    ]
    barrier = pltpu.get_barrier_semaphore()
    pl.semaphore_signal(barrier, inc=1, device_id={"tp": lo_peer}, device_id_type=MESH)
    pl.semaphore_signal(barrier, inc=1, device_id={"tp": hi_peer}, device_id_type=MESH)

    @pl.loop(1, n_ep)
    def _(j):
        pl.semaphore_signal(barrier, inc=1, device_id={"ep": lax.rem(me + j, n_ep)}, device_id_type=MESH)

    for load in loads:
        load.start()
    pl.semaphore_wait(barrier, 2 + n_ep - 1)

    n_hi = remote(normed_ref, seg.at[t], ns.at[0], nr.at[0], {"tp": hi_peer})
    n_lo = remote(normed_ref, seg.at[t], ns.at[1], nr.at[1], {"tp": lo_peer})
    n_relay = remote(seg.at[hi_peer], seg.at[hi_peer], ns.at[2], nr.at[2], {"tp": lo_peer})
    n_hi.start()
    n_lo.start()

    def copy_a(j):
        to = lax.rem(me - j + n_ep, n_ep)
        return remote(outgoing_ref.at[to], rows.at[j, t], as_.at[j], ar.at[j], {"ep": to})

    def copy_b_hi(j, src):
        return remote(src, rows.at[j, t], bs.at[0, j], br.at[0, j], {"tp": hi_peer})

    def copy_b_lo(j, src):
        return remote(src, rows.at[j, t], bs.at[1, j], br.at[1, j], {"tp": lo_peer})

    def copy_c(j):
        return remote(rows.at[j, hi_peer], rows.at[j, hi_peer], cs.at[j], cr.at[j], {"tp": lo_peer})

    def copy_d(j, h):
        return remote(res.at[j, 2 * h + (1 - lo)], drec.at[j, h], ds.at[h, j], dr.at[h, j], {"tp": lo_peer})

    def copy_e(j):
        return remote(drec.at[j, other_hi], erec.at[j], es.at[j], er.at[j], {"tp": hi_peer})

    def copy_f(j):
        to = lax.rem(me + j, n_ep)
        return remote(fin.at[j], returned_ref.at[me], fs.at[j], fr.at[j], {"ep": to})

    def copy_kv(b):
        return remote(kv.at[b], kv.at[b], ks.at[b], kr.at[b], {"ep": lax.rem(me + 1, n_ep)})

    @pl.loop(1, n_ep)
    def _(j):
        copy_a(j).start()

    copy_b_hi(0, outgoing_ref.at[me]).start()
    copy_b_lo(0, outgoing_ref.at[me]).start()
    seg[t] = normed_ref[...]
    rows[0, t] = outgoing_ref[me]

    n_hi.wait_recv()
    n_relay.start()
    for load in loads[:3]:
        load.wait()
    if n_ep > 1:
        copy_a(1).wait_recv()
        copy_b_hi(1, rows.at[1, t]).start()
        copy_b_lo(1, rows.at[1, t]).start()
    n_lo.wait_recv()
    n_relay.wait_recv()

    @pl.loop(0, 2)
    def _(i):
        x = seg[pl.ds(2 * i, 2)].reshape(2 * mix_rows, width)
        r = pl.ds(pl.multiple_of(i * 2 * mix_rows, 2 * mix_rows), 2 * mix_rows)
        kv[me, r, pl.ds(0, head_width)] = jnp.dot(x, wk[...], preferred_element_type=F32).astype(BF16)
        kv[me, r, pl.ds(head_width, head_width)] = jnp.dot(x, wv[...], preferred_element_type=F32).astype(BF16)
        queries[r, :] = jnp.dot(x, wq[...], preferred_element_type=F32).astype(BF16)

    @pl.when(me + 1 < n_ep)
    def _():
        copy_kv(me).start()

    copy_b_hi(0, outgoing_ref.at[me]).wait_recv()
    copy_c(0).start()
    for load in loads[4:]:
        load.wait()

    f_width = eg.shape[1]
    f_tile = tile_of(f_width, 256)
    d_tile = tile_of(width, 512)

    def step_e(j):
        copy_d(j, 0).wait_recv()
        copy_d(j, 1).wait_recv()
        drec[j, other_hi] = (res[j, hi_peer].astype(F32) + drec[j, other_hi].astype(F32)).astype(BF16)
        copy_e(j).start()

    def step_f(j):
        copy_e(j).wait_recv()
        total = (res[j, t].astype(F32) + drec[j, hi].astype(F32) + erec[j].astype(F32)).astype(BF16)

        @pl.when(j == 0)
        def _():
            returned_ref[me] = total

        @pl.when(j > 0)
        def _():
            fin[j] = total
            copy_f(j).start()

    @pl.loop(0, n_ep)
    def _(j):
        @pl.when(j + 2 < n_ep)
        def _():
            copy_a(j + 2).wait_recv()
            copy_b_hi(j + 2, rows.at[j + 2, t]).start()
            copy_b_lo(j + 2, rows.at[j + 2, t]).start()

        @pl.when(j + 1 < n_ep)
        def _():
            copy_b_hi(j + 1, rows.at[j + 1, t]).wait_recv()
            copy_c(j + 1).start()

        @pl.when((j >= 1) & (me - j >= 0))
        def _():
            copy_kv(me - j).wait_recv()

            @pl.when(me + 1 < n_ep)
            def _():
                copy_kv(me - j).start()

        copy_b_lo(j, rows.at[j, t]).wait_recv()
        copy_c(j).wait_recv()

        @pl.loop(0, f_width // f_tile)
        def _(f):
            x = rows[j].reshape(4 * cap, width)
            c = pl.ds(pl.multiple_of(f * f_tile, f_tile), f_tile)
            g = jnp.dot(x, eg[:, c], preferred_element_type=F32)
            u = jnp.dot(x, eu[:, c], preferred_element_type=F32)
            hid[:, c] = (g / (1.0 + jnp.exp(-g)) * u).astype(BF16)

        @pl.loop(0, width // d_tile)
        def _(d):
            c = pl.ds(pl.multiple_of(d * d_tile, d_tile), d_tile)
            y = jnp.dot(hid[...], ed[:, c], preferred_element_type=F32)
            res[j, :, :, c] = y.astype(BF16).reshape(4, cap, d_tile)

        copy_d(j, 0).start()
        copy_d(j, 1).start()

        @pl.when(j >= 1)
        def _():
            step_e(j - 1)

        @pl.when(j >= 2)
        def _():
            step_f(j - 2)

    step_e(n_ep - 1)
    if n_ep > 1:
        step_f(n_ep - 2)

    scale = head_dim ** (-0.5)
    q_tile = span // 2
    for h in range(heads):
        hc = pl.ds(h * head_dim, head_dim)
        vc = pl.ds(head_width + h * head_dim, head_dim)

        @pl.loop(0, 2)
        def _(i):
            r = pl.ds(pl.multiple_of(i * q_tile, q_tile), q_tile)
            run_max[...] = jnp.full_like(run_max, MASKED)
            run_sum[...] = jnp.zeros_like(run_sum)
            run_acc[...] = jnp.zeros_like(run_acc)

            def block(b, masked):
                kc = pl.ds(pl.multiple_of(b * span, span), span)
                s = lax.dot_general(
                    queries[r, hc], kv[b, :, hc], (((1,), (1,)), ((), ())), preferred_element_type=F32
                )
                s = s * scale + query_gate_ref[r, h : h + 1] - gate_ref[h : h + 1, kc]
                if masked:
                    row = lax.broadcasted_iota(jnp.int32, s.shape, 0) + i * q_tile
                    col = lax.broadcasted_iota(jnp.int32, s.shape, 1)
                    s = jnp.where(col <= row, s, MASKED)
                old = run_max[...]
                new = jnp.maximum(old, jnp.max(s, axis=1, keepdims=True))
                w = jnp.exp(s - new)
                fix = jnp.exp(old - new)
                run_max[...] = new
                run_sum[...] = run_sum[...] * fix + jnp.sum(w, axis=1, keepdims=True)
                run_acc[...] = run_acc[...] * fix + jnp.dot(
                    w.astype(BF16), kv[b, :, vc], preferred_element_type=F32
                )

            block(me, True)

            @pl.loop(0, me)
            def _(b):
                block(b, False)

            attended[r, hc] = (run_acc[...] / run_sum[...]).astype(BF16)

    loads[3].wait()
    n_relay.wait_send()
    part = seg

    def project(b):
        x = attended[pl.ds(pl.multiple_of(b * mix_rows, mix_rows), mix_rows), :]

        @pl.loop(0, width // d_tile)
        def _(d):
            c = pl.ds(pl.multiple_of(d * d_tile, d_tile), d_tile)
            part[b, :, c] = jnp.dot(x, wo[:, c], preferred_element_type=F32).astype(BF16)

    def copy_m(h):
        return remote(part.at[2 * h + (1 - lo)], mdrec.at[h], ms.at[h], mr.at[h], {"tp": lo_peer})

    m_hi = remote(mdrec.at[other_hi], merec, ms.at[2], mr.at[2], {"tp": hi_peer})
    project(2 * other_hi + (1 - lo))
    copy_m(other_hi).start()
    project(hi_peer)
    project(lo_peer)
    copy_m(hi).start()
    copy_m(other_hi).wait_recv()
    mdrec[other_hi] = (part[hi_peer].astype(F32) + mdrec[other_hi].astype(F32)).astype(BF16)
    m_hi.start()
    project(t)
    step_f(n_ep - 1)
    copy_m(hi).wait_recv()
    m_hi.wait_recv()
    total = part[t].astype(F32) + mdrec[hi].astype(F32) + merec[...].astype(F32)
    inverse = lax.rsqrt(jnp.mean(total * total, axis=-1, keepdims=True) + EPS)
    mixer_ref[...] = (total * inverse * post_gain_ref[...]).astype(BF16)

    n_hi.wait_send()
    n_lo.wait_send()
    copy_m(0).wait_send()
    copy_m(1).wait_send()
    m_hi.wait_send()

    @pl.loop(0, n_ep)
    def _(j):
        @pl.when(j > 0)
        def _():
            copy_a(j).wait_send()
            copy_f(j).wait_send()
            copy_f(j).wait_recv()

        copy_b_hi(j, rows.at[j, t]).wait_send()
        copy_b_lo(j, rows.at[j, t]).wait_send()
        copy_c(j).wait_send()
        copy_d(j, 0).wait_send()
        copy_d(j, 1).wait_send()
        copy_e(j).wait_send()

        @pl.when((j <= me) & (me + 1 < n_ep))
        def _():
            copy_kv(j).wait_send()


def on_device(
    mixer_input,
    forget_cumsum,
    mixer_gain,
    query_weight,
    key_weight,
    value_weight,
    out_weight,
    post_gain,
    expert_input,
    expert_gain,
    routes,
    route_weight,
    expert_gate,
    expert_upward,
    expert_down,
):
    n_ep = lax.axis_size("ep")
    n_tp = lax.axis_size("tp")
    mix_rows, width = mixer_input.shape
    heads = forget_cumsum.shape[0]
    head_width = query_weight.shape[1]
    head_dim = head_width // heads
    span = mix_rows * n_tp
    moe_rows, top_count = routes.shape
    experts_local = expert_gate.shape[0]
    assert n_tp == 4 and experts_local == 1
    experts_all = n_ep
    capacity = (moe_rows * top_count * 9 + 8 * experts_all - 1) // (8 * experts_all)
    cap = (capacity + ROW_TILE - 1) // ROW_TILE * ROW_TILE
    slots_all = experts_all * cap
    first_pos = lax.axis_index("ep") * span

    normed = normalize(mixer_input, mixer_gain).astype(BF16)
    normed_moe = normalize(expert_input, expert_gain).astype(BF16)
    flat_routes = routes.reshape(-1)
    member = (flat_routes[:, None] == jnp.arange(experts_all, dtype=jnp.int32)[None, :]).astype(F32)
    order = jnp.arange(moe_rows * top_count, dtype=jnp.int32)
    earlier = (order[None, :] < order[:, None]).astype(BF16)
    before = jnp.dot(earlier, member.astype(BF16), preferred_element_type=F32)
    slot_rank = jnp.sum(before * member, axis=1).astype(jnp.int32)
    slot_index = (flat_routes * cap + slot_rank).reshape(moe_rows, top_count)
    slot_ids = jnp.arange(slots_all, dtype=jnp.int32)
    choosers = [
        (slot_index[:, which][:, None] == slot_ids[None, :]).astype(BF16) for which in range(top_count)
    ]
    dispatch = functools.reduce(lambda a, b: a + b, choosers)
    outgoing = lax.dot_general(
        dispatch, normed_moe, (((0,), (0,)), ((), ())), preferred_element_type=F32
    ).astype(BF16)
    outgoing = outgoing.reshape(n_ep, cap, width)
    query_gate = lax.dynamic_slice_in_dim(forget_cumsum, first_pos, span, 1).T

    vmem = pl.BlockSpec(memory_space=pltpu.VMEM)
    hbm = pl.BlockSpec(memory_space=pl.ANY)
    dma = pltpu.SemaphoreType.DMA
    f_width = expert_gate.shape[2]
    mixer_output, returned = pl.pallas_call(
        functools.partial(kernel, n_ep, head_dim),
        out_shape=(
            jax.ShapeDtypeStruct((mix_rows, width), BF16),
            jax.ShapeDtypeStruct((n_ep, cap, width), BF16),
        ),
        in_specs=[vmem] * 5 + [hbm] * 7,
        out_specs=(vmem, vmem),
        scratch_shapes=[
            pltpu.VMEM((width, head_width), BF16),
            pltpu.VMEM((width, head_width), BF16),
            pltpu.VMEM((width, head_width), BF16),
            pltpu.VMEM((head_width, width), BF16),
            pltpu.VMEM((width, f_width), BF16),
            pltpu.VMEM((width, f_width), BF16),
            pltpu.VMEM((f_width, width), BF16),
            pltpu.VMEM((4, mix_rows, width), BF16),
            pltpu.VMEM((span, head_width), BF16),
            pltpu.VMEM((n_ep, span, 2 * head_width), BF16),
            pltpu.VMEM((n_ep, 4, cap, width), BF16),
            pltpu.VMEM((4 * cap, f_width), BF16),
            pltpu.VMEM((n_ep, 4, cap, width), BF16),
            pltpu.VMEM((n_ep, 2, cap, width), BF16),
            pltpu.VMEM((n_ep, cap, width), BF16),
            pltpu.VMEM((n_ep, cap, width), BF16),
            pltpu.VMEM((span // 2, 1), F32),
            pltpu.VMEM((span // 2, 1), F32),
            pltpu.VMEM((span // 2, head_dim), F32),
            pltpu.VMEM((span, head_width), BF16),
            pltpu.VMEM((2, mix_rows, width), BF16),
            pltpu.VMEM((mix_rows, width), BF16),
            dma((7,)),
            dma((3,)),
            dma((3,)),
            dma((n_ep,)),
            dma((n_ep,)),
            dma((2, n_ep)),
            dma((2, n_ep)),
            dma((n_ep,)),
            dma((n_ep,)),
            dma((2, n_ep)),
            dma((2, n_ep)),
            dma((n_ep,)),
            dma((n_ep,)),
            dma((n_ep,)),
            dma((n_ep,)),
            dma((n_ep,)),
            dma((n_ep,)),
            dma((3,)),
            dma((3,)),
        ],
        compiler_params=pltpu.CompilerParams(
            collective_id=0, has_side_effects=True, vmem_limit_bytes=66_500_000
        ),
    )(
        normed,
        outgoing,
        query_gate,
        forget_cumsum,
        post_gain.reshape(1, -1),
        query_weight,
        key_weight,
        value_weight,
        out_weight,
        expert_gate[0],
        expert_upward[0],
        expert_down[0],
    )
    returned = returned.reshape(slots_all, width)
    combined = jnp.zeros((moe_rows, width), F32)
    for which in range(top_count):
        picked = jnp.dot(choosers[which], returned, preferred_element_type=F32)
        combined = combined + route_weight[:, which : which + 1] * picked
    return (mixer_output, combined.astype(BF16))


ROW_TILE = 16


def solution(mesh):
    rows = P(("grp", "ep", "tp"), None)
    in_specs = (
        rows,
        P("tp", "grp"),
        P(),
        P(None, "tp"),
        P(None, "tp"),
        P(None, "tp"),
        P("tp", None),
        P(),
        rows,
        P(),
        rows,
        rows,
        P("ep", None, "tp"),
        P("ep", None, "tp"),
        P("ep", "tp", None),
    )
    return jax.shard_map(
        on_device, mesh=mesh, in_specs=in_specs, out_specs=(rows, rows), check_vma=False
    )
```

time: 286 us -> 126 us (0.44); the launches traced: 282 us -> 126 us
  waiting for transfers between devices: 174 us -> 0 us
  Pallas kernels: 0 us -> 113 us
  matrix products: 52.8 us -> 5.76 us
  between operations: 14 us -> 0.76 us
  starting transfers between devices: 11.6 us -> 0 us
  other arithmetic: 14.3 us -> 3.12 us
  local copies, waits for them, and re-layouts: 14.6 us -> 3.56 us
    pallas_call x0 -> x1, Pallas kernels: none -> 113 us  [on_device(): pl.pallas_call(functools.partial(kernel, n_ep, head_dim), out_shape=(jax....]
    all_to_all x2 -> x0, waiting for transfers between devices: 77.5 us -> none  [the longest x1 77.5 us: on_device(): lax.all_to_all(copies, ('ep', 'tp'), split_axis=0, concat_axis=0, tiled=T...]
    reduce_scatter x2 -> x0, waiting for transfers between devices: 52.1 us -> none  [the longest x1 28.5 us: on_device(): lax.psum_scatter(jnp.dot(selected, out_weight, preferred_element_type=jnp...]
    dot_general x22 -> x3, matrix products: 51.2 us -> 3.38 us  [the longest x2 3.18 us: on_device(): picked = jnp.dot(choosers[which], returned, preferred_element_type=F32)]
    all_gather x3 -> x0, waiting for transfers between devices: 44.8 us -> none  [the longest x1 44.8 us: on_device(): segment = lax.all_gather(normed, 'tp', axis=0, tiled=True)]
    all_to_all x2 -> x0, starting transfers between devices: 11.2 us -> none  [the longest x1 6.15 us: on_device(): lax.all_to_all(copies, ('ep', 'tp'), split_axis=0, concat_axis=0, tiled=T...]
    dynamic_slice x9 -> x1, local copies, waits for them, and re-layouts: 4.66 us -> 0.75 us  [on_device(): query_gate = lax.dynamic_slice_in_dim(forget_cumsum, first_pos, span, 1).T]
    concatenate x1 -> x0, other arithmetic: 3.85 us -> none  [on_device(): jnp.concatenate(pieces, axis=0).astype(jnp.bfloat16)]
  transfers between devices with their start and end apart: 7 -> 0, of which waited for: 4 -> 0; matrix products, arithmetic and copies ran while one was open for 25% -> 0% of each run, Pallas kernels for 0% -> 0%
where the time goes in v1:
time: 126 us
  Pallas kernels  113 us (90%)
  matrix products  5.76 us (5%)
  local copies, waits for them, and re-layouts  3.56 us (3%)
  other arithmetic  3.12 us (2%)
    pallas_call x1, Pallas kernels, on_device(): pl.pallas_call(functools.partial(kernel, n_ep, head_dim), out_shape=(jax....  113 us
    dot_general x2, matrix products, on_device(): picked = jnp.dot(choosers[which], returned, preferred_element_type=F32)  3.18 us

profile of v1, /device:TPU:26, one launch (start us, length us, event | category | flops | bytes accessed | tf_op | source)
XLA Modules:
  0.0 126.0 jit_solution(12535378114456216009)
XLA Ops:
  0.6 0.0 copy-start.2
  0.6 0.7 constant_dynamic-slice_fusion
  1.4 0.9 copy.29
  2.3 0.8 copy.26
  3.0 0.1 eq.45
  3.2 0.0 copy-start.1
  3.2 0.2 fusion.2
  3.4 0.1 convert_element_type.43
  3.5 0.1 copy.27
  3.6 0.7 multiply_add_fusion
  4.3 1.2 fusion.6
  5.5 0.0 copy-start.4
  5.6 0.0 copy-done.2
  5.6 2.4 %convolution_convert_fusion = bf16[320,2048]{1,0:T(8,128)(2,1)} fusion(bf16[128,2048]{1,0:T(8,128)(2,1)S(1)} %copy-done.2, f32[2048]{0:T(1024)} %param.24, f32[128]{0:T(128)S(1)} %add_rsqrt_fusion, s32[128]{0:T(128)S(1)} %get-tuple-element.9, s32[128]{0:T(128)S(1)} %get-tuple-element.8), kind=kOutput, calls=%fused_computation | convolution fusion | flops 169803776 | bytes 1844736 | tf_op jit(solution)/shard_map/dot_general | solution.py:418
  8.0 0.0 copy-done.1
  8.0 0.2 fusion.3
  8.2 0.0 copy-done.4
  8.2 1.0 fusion.5.normed_ref
  9.2 0.0 copy-start.5
  9.2 112.8 %shard_map.158 = (bf16[128,2048]{1,0:T(8,128)(2,1)}, bf16[4,80,2048]{2,1,0:T(8,128)(2,1)}) custom-call(bf16[128,2048]{1,0:T(8,128)(2,1)} %fusion.5.normed_ref, bf16[4,80,2048]{2,1,0:T(8,128)(2,1)} %bitcast.19, f32[512,2]{1,0:T(8,128)} %bitcast.23, f32[2,2048]{1,0:T(2,128)} %gate_ref.1, f32[1,2048]{1,0:T(1,128)} %bitcast.24, bf16[2048,256]{1,0:T(8,128)(2,1)} %wq_hbm.1, ...), custom_call_target="tpu_custom_call" | custom-call | tf_op jit(solution)/shard_map/pallas_call | solution.py:428
  121.9 0.0 copy-start
  122.0 0.0 copy-done.5
  122.0 1.9 %convolution_multiply_fusion.1 = f32[128,2048]{1,0:T(8,128)S(1)} fusion(bf16[320,2048]{1,0:T(8,128)(2,1)} %bitcast.17, f32[128]{0:T(128)S(1)} %get-tuple-element.7, s32[128]{0:T(128)S(1)} %get-tuple-element.8), kind=kOutput, calls=%fused_computation.3 | convolution fusion | flops 168075264 | bytes 2360320 | tf_op jit(solution)/shard_map/dot_general | solution.py:499
  123.9 0.0 copy-done
  123.9 0.0 copy-start.3
  123.9 1.3 %fusion.1 = bf16[128,2048]{1,0:T(8,128)(2,1)} fusion(f32[128,2048]{1,0:T(8,128)S(1)} %convolution_multiply_fusion.1, bf16[320,2048]{1,0:T(8,128)(2,1)S(1)} %bitcast.18, f32[128]{0:T(128)S(1)} %get-tuple-element.6, s32[128]{0:T(128)S(1)} %get-tuple-element.9), kind=kOutput, calls=%fused_computation.4 | convolution fusion | flops 168599552 | bytes 2884608 | tf_op jit(solution)/shard_map/dot_general | solution.py:499
  125.2 0.0 copy-done.3
  125.2 0.8 copy.31
  (5 shorter events, 0.0 us)
Async XLA Ops:
  0.6 4.9 %copy-start.2 = (bf16[128,2048]{1,0:T(8,128)(2,1)S(1)}, bf16[128,2048]{1,0:T(8,128)(2,1)}, u32[]{:S(2)}) copy-start(bf16[128,2048]{1,0:T(8,128)(2,1)} %param.23) | copy-start | bytes 1572868
  3.2 4.8 %copy-start.1 = (bf16[128,2048]{1,0:T(8,128)(2,1)S(1)}, bf16[128,2048]{1,0:T(8,128)(2,1)}, u32[]{:S(2)}) copy-start(bf16[128,2048]{1,0:T(8,128)(2,1)} %param.15) | copy-start | bytes 1572868
  5.5 2.6 %copy-start.4 = (f32[2048]{0:T(1024)S(1)}, f32[2048]{0:T(1024)}, u32[]{:S(2)}) copy-start(f32[2048]{0:T(1024)} %param.17) | copy-start | bytes 24580
  9.2 112.8 %copy-start.5 = (f32[128,2]{0,1:T(2,128)S(1)}, f32[128,2]{0,1:T(2,128)}, u32[]{:S(2)}) copy-start(f32[128,2]{0,1:T(2,128)} %param.26) | copy-start | bytes 3076
  121.9 1.9 %copy-start = (bf16[4,80,2048]{2,1,0:T(8,128)(2,1)S(1)}, bf16[4,80,2048]{2,1,0:T(8,128)(2,1)}, u32[]{:S(2)}) copy-start(bf16[4,80,2048]{2,1,0:T(8,128)(2,1)} %get-tuple-element.5) | copy-start | bytes 3932164
  123.9 1.3 %copy-start.3 = (bf16[128,2048]{1,0:T(8,128)(2,1)S(1)}, bf16[128,2048]{1,0:T(8,128)(2,1)}, u32[]{:S(2)}) copy-start(bf16[128,2048]{1,0:T(8,128)(2,1)} %get-tuple-element.12) | copy-start | bytes 1572868

commit v2 on v1

--- a/solution.py
+++ b/solution.py
@@ -229,14 +229,6 @@
             copy_b_hi(j + 1, rows.at[j + 1, t]).wait_recv()
             copy_c(j + 1).start()
 
-        @pl.when((j >= 1) & (me - j >= 0))
-        def _():
-            copy_kv(me - j).wait_recv()
-
-            @pl.when(me + 1 < n_ep)
-            def _():
-                copy_kv(me - j).start()
-
         copy_b_lo(j, rows.at[j, t]).wait_recv()
         copy_c(j).wait_recv()
 
@@ -261,29 +253,31 @@
         def _():
             step_e(j - 1)
 
-        @pl.when(j >= 2)
-        def _():
-            step_f(j - 2)
+        @pl.when((j >= 1) & (j < n_ep - 1) & (me - j >= 0))
+        def _():
+            copy_kv(me - j).wait_recv()
+
+            @pl.when(me + 1 < n_ep)
+            def _():
+                copy_kv(me - j).start()
 
     step_e(n_ep - 1)
-    if n_ep > 1:
-        step_f(n_ep - 2)
 
     scale = head_dim ** (-0.5)
     q_tile = span // 2
-    for h in range(heads):
-        hc = pl.ds(h * head_dim, head_dim)
-        vc = pl.ds(head_width + h * head_dim, head_dim)
-
-        @pl.loop(0, 2)
-        def _(i):
-            r = pl.ds(pl.multiple_of(i * q_tile, q_tile), q_tile)
-            run_max[...] = jnp.full_like(run_max, MASKED)
-            run_sum[...] = jnp.zeros_like(run_sum)
-            run_acc[...] = jnp.zeros_like(run_acc)
-
-            def block(b, masked):
-                kc = pl.ds(pl.multiple_of(b * span, span), span)
+    run_max[...] = jnp.full_like(run_max, MASKED)
+    run_sum[...] = jnp.zeros_like(run_sum)
+    run_acc[...] = jnp.zeros_like(run_acc)
+
+    def attend(b, masked):
+        kc = pl.ds(pl.multiple_of(b * span, span), span)
+        for h in range(heads):
+            hc = pl.ds(h * head_dim, head_dim)
+            vc = pl.ds(head_width + h * head_dim, head_dim)
+
+            @pl.loop(0, 2)
+            def _(i):
+                r = pl.ds(pl.multiple_of(i * q_tile, q_tile), q_tile)
                 s = lax.dot_general(
                     queries[r, hc], kv[b, :, hc], (((1,), (1,)), ((), ())), preferred_element_type=F32
                 )
@@ -292,23 +286,35 @@
                     row = lax.broadcasted_iota(jnp.int32, s.shape, 0) + i * q_tile
                     col = lax.broadcasted_iota(jnp.int32, s.shape, 1)
                     s = jnp.where(col <= row, s, MASKED)
-                old = run_max[...]
+                old = run_max[h, r]
                 new = jnp.maximum(old, jnp.max(s, axis=1, keepdims=True))
                 w = jnp.exp(s - new)
                 fix = jnp.exp(old - new)
-                run_max[...] = new
-                run_sum[...] = run_sum[...] * fix + jnp.sum(w, axis=1, keepdims=True)
-                run_acc[...] = run_acc[...] * fix + jnp.dot(
+                run_max[h, r] = new
+                run_sum[h, r] = run_sum[h, r] * fix + jnp.sum(w, axis=1, keepdims=True)
+                run_acc[h, r] = run_acc[h, r] * fix + jnp.dot(
                     w.astype(BF16), kv[b, :, vc], preferred_element_type=F32
                 )
 
-            block(me, True)
-
-            @pl.loop(0, me)
-            def _(b):
-                block(b, False)
-
-            attended[r, hc] = (run_acc[...] / run_sum[...]).astype(BF16)
+    attend(me, True)
+    if n_ep > 2:
+
+        @pl.loop(0, n_ep - 2)
+        def _(j):
+            step_f(j)
+
+    @pl.loop(1, me + 1)
+    def _(d):
+        @pl.when(d == n_ep - 1)
+        def _():
+            copy_kv(0).wait_recv()
+
+        attend(me - d, False)
+
+    for h in range(heads):
+        attended[:, pl.ds(h * head_dim, head_dim)] = (run_acc[h] / run_sum[h]).astype(BF16)
+    if n_ep > 1:
+        step_f(n_ep - 2)
 
     loads[3].wait()
     n_relay.wait_send()
@@ -450,9 +456,9 @@
             pltpu.VMEM((n_ep, 2, cap, width), BF16),
             pltpu.VMEM((n_ep, cap, width), BF16),
             pltpu.VMEM((n_ep, cap, width), BF16),
-            pltpu.VMEM((span // 2, 1), F32),
-            pltpu.VMEM((span // 2, 1), F32),
-            pltpu.VMEM((span // 2, head_dim), F32),
+            pltpu.VMEM((heads, span, 1), F32),
+            pltpu.VMEM((heads, span, 1), F32),
+            pltpu.VMEM((heads, span, head_dim), F32),
             pltpu.VMEM((span, head_width), BF16),
             pltpu.VMEM((2, mix_rows, width), BF16),
             pltpu.VMEM((mix_rows, width), BF16),
@@ -501,7 +507,7 @@
     return (mixer_output, combined.astype(BF16))
 
 
-ROW_TILE = 16
+ROW_TILE = 8
 
 
 def solution(mesh):

time: 126 us -> 105 us (0.83)
  the two profiles are of different devices: /device:TPU:26 before, /device:TPU:9 now
where the time goes in v2:
time: 105 us
  Pallas kernels  92 us (88%)
  matrix products  5.62 us (5%)
  local copies, waits for them, and re-layouts  3.56 us (3%)
  other arithmetic  3.12 us (3%)
    pallas_call x1, Pallas kernels, on_device(): pl.pallas_call(functools.partial(kernel, n_ep, head_dim), out_shape=(jax....  92 us
    dot_general x2, matrix products, on_device(): picked = jnp.dot(choosers[which], returned, preferred_element_type=F32)  3.13 us
    unnamed x15, local copies, waits for them, and re-layouts  2.47 us
    dot_general x1, matrix products, on_device(): lax.dot_general(dispatch, normed_moe, (((0,), (0,)), ((), ())), preferred...  2.29 us

profile of v2, /device:TPU:9, one launch (start us, length us, event | category | flops | bytes accessed | tf_op | source)
XLA Modules:
  0.0 105.0 jit_solution(12674636994763980484)
XLA Ops:
  0.6 0.0 copy-start.1
  0.6 0.7 constant_dynamic-slice_fusion
  1.4 0.9 copy.29
  2.3 0.8 copy.26
  3.0 0.1 eq.45
  3.2 0.2 fusion.2
  3.4 0.0 copy-start.2
  3.4 0.1 convert_element_type.43
  3.6 0.1 copy.27
  3.6 0.7 multiply_add_fusion
  4.3 1.2 %fusion.6 = f32[128]{0:T(128)S(1)} fusion(bf16[128,2048]{1,0:T(8,128)(2,1)} %param.23), kind=kLoop, calls=%fused_computation.14 | loop fusion | flops 786304 | bytes 524800 | tf_op jit(solution)/shard_map/reduce_sum | solution.py:19
  5.6 0.0 copy-start.4
  5.6 0.0 copy-done.1
  5.6 2.3 %convolution_convert_fusion = bf16[288,2048]{1,0:T(8,128)(2,1)} fusion(bf16[128,2048]{1,0:T(8,128)(2,1)S(1)} %copy-done.1, f32[2048]{0:T(1024)} %param.24, f32[128]{0:T(128)S(1)} %add_rsqrt_fusion, s32[128]{0:T(128)S(1)} %get-tuple-element.9, s32[128]{0:T(128)S(1)} %get-tuple-element.8), kind=kOutput, calls=%fused_computation | convolution fusion | flops 152928256 | bytes 1713664 | tf_op jit(solution)/shard_map/dot_general | solution.py:424
  7.9 0.0 copy-done.2
  7.9 0.2 fusion.3
  8.1 0.0 copy-done.4
  8.1 1.0 fusion.5.normed_ref
  9.1 0.0 copy-start.5
  9.1 92.0 %shard_map.158 = (bf16[128,2048]{1,0:T(8,128)(2,1)}, bf16[4,72,2048]{2,1,0:T(8,128)(2,1)}) custom-call(bf16[128,2048]{1,0:T(8,128)(2,1)} %fusion.5.normed_ref, bf16[4,72,2048]{2,1,0:T(8,128)(2,1)} %bitcast.19, f32[512,2]{1,0:T(8,128)} %bitcast.23, f32[2,2048]{1,0:T(2,128)} %gate_ref.1, f32[1,2048]{1,0:T(1,128)} %bitcast.24, bf16[2048,256]{1,0:T(8,128)(2,1)} %wq_hbm.1, ...), custom_call_target="tpu_custom_call" | custom-call | tf_op jit(solution)/shard_map/pallas_call | solution.py:434
  101.0 0.0 copy-start
  101.0 0.0 copy-done.5
  101.1 1.8 %convolution_multiply_fusion.1 = f32[128,2048]{1,0:T(8,128)S(1)} fusion(bf16[288,2048]{1,0:T(8,128)(2,1)} %bitcast.17, f32[128]{0:T(128)S(1)} %get-tuple-element.7, s32[128]{0:T(128)S(1)} %get-tuple-element.8), kind=kOutput, calls=%fused_computation.3 | convolution fusion | flops 151293952 | bytes 2229248 | tf_op jit(solution)/shard_map/dot_general | solution.py:505
  102.9 0.0 copy-done
  102.9 0.0 copy-start.3
  102.9 1.3 %fusion.1 = bf16[128,2048]{1,0:T(8,128)(2,1)} fusion(f32[128,2048]{1,0:T(8,128)S(1)} %convolution_multiply_fusion.1, bf16[288,2048]{1,0:T(8,128)(2,1)S(1)} %bitcast.18, f32[128]{0:T(128)S(1)} %get-tuple-element.6, s32[128]{0:T(128)S(1)} %get-tuple-element.9), kind=kOutput, calls=%fused_computation.4 | convolution fusion | flops 151818240 | bytes 2753536 | tf_op jit(solution)/shard_map/dot_general | solution.py:505
  104.2 0.0 copy-done.3
  104.2 0.8 copy.31
  (5 shorter events, 0.0 us)
Async XLA Ops:
  0.6 4.9 %copy-start.1 = (bf16[128,2048]{1,0:T(8,128)(2,1)S(1)}, bf16[128,2048]{1,0:T(8,128)(2,1)}, u32[]{:S(2)}) copy-start(bf16[128,2048]{1,0:T(8,128)(2,1)} %param.23) | copy-start | bytes 1572868
  3.4 4.5 %copy-start.2 = (bf16[128,2048]{1,0:T(8,128)(2,1)S(1)}, bf16[128,2048]{1,0:T(8,128)(2,1)}, u32[]{:S(2)}) copy-start(bf16[128,2048]{1,0:T(8,128)(2,1)} %param.15) | copy-start | bytes 1572868
  5.6 2.5 %copy-start.4 = (f32[2048]{0:T(1024)S(1)}, f32[2048]{0:T(1024)}, u32[]{:S(2)}) copy-start(f32[2048]{0:T(1024)} %param.17) | copy-start | bytes 24580
  9.1 92.0 %copy-start.5 = (f32[128,2]{0,1:T(2,128)S(1)}, f32[128,2]{0,1:T(2,128)}, u32[]{:S(2)}) copy-start(f32[128,2]{0,1:T(2,128)} %param.26) | copy-start | bytes 3076
  101.0 1.9 %copy-start = (bf16[4,72,2048]{2,1,0:T(8,128)(2,1)S(1)}, bf16[4,72,2048]{2,1,0:T(8,128)(2,1)}, u32[]{:S(2)}) copy-start(bf16[4,72,2048]{2,1,0:T(8,128)(2,1)} %get-tuple-element.5) | copy-start | bytes 3538948
  102.9 1.3 %copy-start.3 = (bf16[128,2048]{1,0:T(8,128)(2,1)S(1)}, bf16[128,2048]{1,0:T(8,128)(2,1)}, u32[]{:S(2)}) copy-start(bf16[128,2048]{1,0:T(8,128)(2,1)} %get-tuple-element.12) | copy-start | bytes 1572868
